TPU v7x, 32 devices: a whole 2x2x4 slice. The times are simulated.
32 devices in a mesh: sp: 4 (over y, x), tp: 8 (over z, core).
Axes of the slice: x: 2, y: 2, z: 4, core: 2. Of those that a mesh axis runs over, the one named last changes fastest.
Arguments:
- tokens: bfloat16 [2048, 4096], P('sp', 'tp'), may hold values from -6 to 6
- pre_gain: float32 [2, 4096], replicated, may hold values from 0.1 to 1.9
- w_value: bfloat16 [2, 4096, 4096], P(None, 'sp', 'tp'), may hold values from -0.09375 to 0.09375
- w_gate: bfloat16 [2, 4096, 4096], P(None, 'sp', 'tp'), may hold values from -0.09375 to 0.09375
- conv_taps: float32 [2, 31, 4096], P(None, None, 'tp'), may hold values from -3.5 to 3.5
- conv_bias: float32 [2, 4096], P(None, 'tp'), may hold values from -3 to 3
- norm_gain: float32 [2, 4096], P(None, 'tp'), may hold values from 0.1 to 1.9
- norm_bias: float32 [2, 4096], P(None, 'tp'), may hold values from -3 to 3
- w_out: bfloat16 [2, 4096, 4096], P(None, 'sp', 'tp'), may hold values from -0.09375 to 0.09375
- post_gain: float32 [2, 4096], P(None, 'tp'), may hold values from 0.1 to 1.9
Outputs:
- stream: bfloat16 [2048, 4096], P('sp', 'tp')
All inputs are finite; a program needn't handle non-finite values.
Results may differ from a plain program's by a relative error of at most 0.009.
Values may be sent and summed in bfloat16 or wider, within the bound.
A program may use at most 64 MiB of HBM per device.

v0:
```python
import jax
import jax.numpy as jnp
from jax import lax
from jax.sharding import PartitionSpec as P


def passed_along(value, axis, steps):
    count = lax.axis_size(axis)
    leading, last = (max(0, -steps), min(count, count - steps))
    return lax.ppermute(value, axis, [(source, source + steps) for source in range(leading, last)])


def shards(
    tokens, pre_gain, w_value, w_gate, conv_taps, conv_bias, norm_gain, norm_bias, w_out, post_gain
):
    layer_count = w_value.shape[0]
    tap_count = conv_taps.shape[1]
    channel_count = conv_taps.shape[2] * lax.axis_size("tp")
    model_width = tokens.shape[1] * lax.axis_size("tp")
    local_rows = tokens.shape[0]
    every_value, every_gate, every_out = (
        lax.all_gather(w_value, "sp", axis=1, tiled=True),
        lax.all_gather(w_gate, "sp", axis=1, tiled=True),
        lax.all_gather(w_out, "sp", axis=1, tiled=True),
    )
    stream = tokens
    for layer_index in range(layer_count):
        gathered = lax.all_gather(stream, "tp", axis=1, tiled=True)
        full_rows = gathered.astype(jnp.float32)
        scale_rows = lax.rsqrt(jnp.mean(full_rows * full_rows, axis=-1, keepdims=True) + 1e-06)
        normed = (full_rows * scale_rows * pre_gain[layer_index]).astype(jnp.bfloat16)
        value_block = every_value[layer_index]
        gate_block = every_gate[layer_index]
        out_block = every_out[layer_index]
        value_proj = jnp.dot(normed, value_block, preferred_element_type=jnp.float32)
        gate_proj = jnp.dot(normed, gate_block, preferred_element_type=jnp.float32)
        glu_out = (value_proj * jax.nn.sigmoid(gate_proj)).astype(jnp.bfloat16)
        earlier = passed_along(glu_out[local_rows - (tap_count - 1) :], "sp", 1)
        padded = jnp.concatenate([earlier, glu_out], axis=0).astype(jnp.float32)
        filtered = jnp.zeros(glu_out.shape, jnp.float32) + conv_bias[layer_index]
        for tap_index in range(tap_count):
            filtered = (
                filtered
                + padded[tap_index : tap_index + local_rows] * conv_taps[layer_index, tap_index]
            )
        channel_sum, channel_square = lax.psum(
            (jnp.sum(filtered, axis=-1), jnp.sum(filtered * filtered, axis=-1)), "tp"
        )
        centre = channel_sum / channel_count
        spread = jnp.maximum(channel_square / channel_count - centre * centre, 0.0)
        shaped = (filtered - centre[:, None]) * lax.rsqrt(spread + 1e-05)[:, None]
        mixed = jax.nn.silu(shaped * norm_gain[layer_index] + norm_bias[layer_index]).astype(
            jnp.bfloat16
        )
        whole_mixed = lax.all_gather(mixed, "tp", axis=1, tiled=True)
        branch_low = jnp.dot(whole_mixed, out_block, preferred_element_type=jnp.float32).astype(
            jnp.bfloat16
        )
        branch = lax.optimization_barrier(branch_low).astype(jnp.float32)
        total = lax.psum(jnp.sum(branch * branch, axis=-1), "tp")
        rescale = lax.rsqrt(total / model_width + 1e-06)[:, None]
        stream = (stream.astype(jnp.float32) + branch * rescale * post_gain[layer_index]).astype(
            jnp.bfloat16
        )
    return stream


def solution(mesh):
    in_specs = (
        P("sp", "tp"),
        P(),
        P(None, "sp", "tp"),
        P(None, "sp", "tp"),
        P(None, None, "tp"),
        P(None, "tp"),
        P(None, "tp"),
        P(None, "tp"),
        P(None, "sp", "tp"),
        P(None, "tp"),
    )
    out_specs = P("sp", "tp")
    return jax.shard_map(shards, mesh=mesh, in_specs=in_specs, out_specs=out_specs, check_vma=False)
```

profile of v0, /device:TPU:0, one launch (start us, length us, event | category | flops | bytes accessed | tf_op | source)
XLA Modules:
  0.0 551.2 jit_solution(2232420375245703278)
XLA Ops:
  6.5 0.0 copy-start.5
  6.5 0.0 copy-start.6
  6.5 0.0 all-gather.8.cloned.1.call-start
  6.6 0.7 all-gather.8.cloned.1.call-update
  7.3 0.0 all-gather.12.cloned.1.call-start
  7.3 0.7 all-gather.12.cloned.1.call-update
  8.0 0.0 all-gather.10.cloned.1.call-start
  8.1 0.7 all-gather.10.cloned.1.call-update
  8.8 0.0 all-gather.16.cloned.1.call-start
  8.8 0.5 all-gather.16.cloned.1.call-update
  9.3 0.0 all-gather.14.cloned.1.call-start
  9.4 0.0 copy-done.5
  9.4 0.0 copy-done.6
  9.4 0.0 copy-done.3
  9.5 0.0 copy-done.4
  9.6 49.0 %all-gather.8.cloned.1.call-done = bf16[512,4096]{1,0:T(8,128)(2,1)} async-done(((bf16[512,512]{1,0:T(8,128)(2,1)}), bf16[512,4096]{1,0:T(8,128)(2,1)}) %all-gather.8.cloned.1.call-update) | async-done | bytes 4194320 | tf_op jit(solution)/shard_map/all_gather | solution.py:28
  58.6 3.1 fusion
  61.7 85.1 %all-gather.12.cloned.1.call-done = bf16[2,4096,512]{2,1,0:T(8,128)(2,1)} async-done(((bf16[2,1024,512]{2,1,0:T(8,128)(2,1)}), bf16[2,4096,512]{2,1,0:T(8,128)(2,1)}) %all-gather.12.cloned.1.call-update) | async-done | bytes 8388624 | tf_op jit(solution)/shard_map/all_gather | solution.py:23
  146.7 6.0 %fusion.21 = f32[512,512]{1,0:T(8,128)S(1)} fusion(bf16[2,4096,512]{2,1,0:T(8,128)(2,1)} %all-gather.12.cloned.1.call-done, bf16[512,4096]{1,0:T(8,128)(2,1)} %all-gather.8.cloned.1.call-done, f32[4096]{0:T(1024)S(1)} %bitcast.122, f32[512]{0:T(512)S(1)} %add_rsqrt_fusion.5), kind=kOutput, calls=%fused_computation.35 | convolution fusion | flops 2156658688 | bytes 9455616 | tf_op jit(solution)/shard_map/dot_general | solution.py:36
  152.7 0.0 copy-start.7
  152.7 83.4 %all-gather.10.cloned.1.call-done = bf16[2,4096,512]{2,1,0:T(8,128)(2,1)} async-done(((bf16[2,1024,512]{2,1,0:T(8,128)(2,1)}), bf16[2,4096,512]{2,1,0:T(8,128)(2,1)}) %all-gather.10.cloned.1.call-update) | async-done | bytes 8388624 | tf_op jit(solution)/shard_map/all_gather | solution.py:22
  236.1 5.8 %fusion.23 = bf16[512,512]{1,0:T(8,128)(2,1)S(1)} fusion(f32[512,512]{1,0:T(8,128)S(1)} %fusion.21, bf16[2,4096,512]{2,1,0:T(8,128)(2,1)} %all-gather.10.cloned.1.call-done, bf16[512,4096]{1,0:T(8,128)(2,1)} %all-gather.8.cloned.1.call-done, f32[4096]{0:T(1024)S(1)} %bitcast.123, f32[512]{0:T(512)S(1)} %add_rsqrt_fusion.5), kind=kOutput, calls=%fused_computation.37 | convolution fusion | flops 2156396544 | bytes 9979904 | tf_op jit(solution)/shard_map/dot_general | solution.py:35
  242.0 3.4 collective-permute-start
  245.4 0.0 copy-done.7
  245.4 1.6 collective-permute-done
  246.9 0.2 maximum_convert_fusion
  247.1 0.0 copy-start.8
  247.1 5.0 fusion.101
  252.1 15.3 %all-reduce.1 = (f32[512]{0:T(512)S(1)}, f32[512]{0:T(512)S(1)}) all-reduce(f32[512]{0:T(512)S(1)} %get-tuple-element.8, f32[512]{0:T(512)S(1)} %get-tuple-element.7), channel_id=1, replica_groups=mesh['sp'=4,'tp'=8] {'tp'}, use_global_device_ids=true, to_apply=%region_4.0 | all-reduce | flops 1024 | bytes 8192 | tf_op jit(solution)/shard_map/psum | solution.py:46
  267.4 1.2 multiply_convert_fusion.1
  268.7 0.0 all-gather.14.cloned.1.call-update
  268.7 0.0 all-gather.18.cloned.1.call-start
  268.7 0.0 copy-done.8
  268.8 0.0 copy-start.2
  268.8 56.5 %all-gather.16.cloned.1.call-done = bf16[2,4096,512]{2,1,0:T(8,128)(2,1)} async-done(((bf16[2,1024,512]{2,1,0:T(8,128)(2,1)}), bf16[2,4096,512]{2,1,0:T(8,128)(2,1)}) %all-gather.16.cloned.1.call-update) | async-done | bytes 8388624 | tf_op jit(solution)/shard_map/all_gather | solution.py:24
  325.3 48.4 %all-gather.14.cloned.1.call-done = bf16[512,4096]{1,0:T(8,128)(2,1)} async-done(((bf16[512,512]{1,0:T(8,128)(2,1)}), bf16[512,4096]{1,0:T(8,128)(2,1)}) %all-gather.14.cloned.1.call-update) | async-done | bytes 4194320 | tf_op jit(solution)/shard_map/all_gather | solution.py:55
  373.7 5.8 %fusion.24 = bf16[512,512]{1,0:T(8,128)(2,1)S(1)} fusion(bf16[512,4096]{1,0:T(8,128)(2,1)} %all-gather.14.cloned.1.call-done, bf16[2,4096,512]{2,1,0:T(8,128)(2,1)} %all-gather.16.cloned.1.call-done), kind=kOutput, calls=%fused_computation.38 | convolution fusion | flops 2147745792 | bytes 8912896 | tf_op jit(solution)/shard_map/dot_general | solution.py:56
  379.5 0.2 fusion.30
  379.6 14.8 %psum.44 = f32[512]{0:T(512)S(1)} all-reduce(f32[512]{0:T(512)S(1)} %fusion.30), channel_id=1, replica_groups=mesh['sp'=4,'tp'=8] {'tp'}, use_global_device_ids=true, to_apply=%region_6.7 | all-reduce | flops 512 | bytes 4096 | tf_op jit(solution)/shard_map/psum | solution.py:60
  394.4 0.0 copy-done.2
  394.5 1.1 fusion.33
  395.5 0.0 all-gather.18.cloned.1.call-update
  395.5 0.2 all-gather.20.cloned.1.call-start
  395.8 44.7 %all-gather.18.cloned.1.call-done = bf16[512,4096]{1,0:T(8,128)(2,1)} async-done(((bf16[512,512]{1,0:T(8,128)(2,1)}), bf16[512,4096]{1,0:T(8,128)(2,1)}) %all-gather.18.cloned.1.call-update) | async-done | bytes 4194320 | tf_op jit(solution)/shard_map/all_gather | solution.py:28
  440.5 3.2 fusion.3
  443.7 0.2 copy-done.1
  443.9 5.0 fusion.19
  448.9 0.0 slice-done
  448.9 0.0 slice-done.1
  449.0 2.4 fusion.22
  451.4 3.4 collective-permute-start.1
  454.9 1.5 collective-permute-done.1
  456.4 0.2 maximum_convert_fusion.1
  456.5 5.0 fusion.100
  461.6 13.7 %all-reduce = (f32[512]{0:T(512)S(1)}, f32[512]{0:T(512)S(1)}) all-reduce(f32[512]{0:T(512)S(1)} %get-tuple-element.6, f32[512]{0:T(512)S(1)} %get-tuple-element.5), channel_id=1, replica_groups=mesh['sp'=4,'tp'=8] {'tp'}, use_global_device_ids=true, to_apply=%region_11.12 | all-reduce | flops 1024 | bytes 8192 | tf_op jit(solution)/shard_map/psum | solution.py:46
  475.3 1.3 multiply_convert_fusion
  476.6 0.0 all-gather.20.cloned.1.call-update
  476.6 0.0 copy-start
  476.6 45.9 %all-gather.20.cloned.1.call-done = bf16[512,4096]{1,0:T(8,128)(2,1)} async-done(((bf16[512,512]{1,0:T(8,128)(2,1)}), bf16[512,4096]{1,0:T(8,128)(2,1)}) %all-gather.20.cloned.1.call-update) | async-done | bytes 4194320 | tf_op jit(solution)/shard_map/all_gather | solution.py:55
  522.5 5.8 %fusion.25 = bf16[512,512]{1,0:T(8,128)(2,1)S(1)} fusion(bf16[512,4096]{1,0:T(8,128)(2,1)} %all-gather.20.cloned.1.call-done, bf16[2,4096,512]{2,1,0:T(8,128)(2,1)} %all-gather.16.cloned.1.call-done), kind=kOutput, calls=%fused_computation.39 | convolution fusion | flops 2147745792 | bytes 8912896 | tf_op jit(solution)/shard_map/dot_general | solution.py:56
  528.3 0.2 fusion.34
  528.5 14.8 %psum.47 = f32[512]{0:T(512)S(1)} all-reduce(f32[512]{0:T(512)S(1)} %fusion.34), channel_id=1, replica_groups=mesh['sp'=4,'tp'=8] {'tp'}, use_global_device_ids=true, to_apply=%region_13.14 | all-reduce | flops 512 | bytes 4096 | tf_op jit(solution)/shard_map/psum | solution.py:60
  543.3 0.0 copy-done
  543.3 1.1 fusion.37
  (23 shorter events, 0.3 us)
Async XLA Ops:
  6.5 2.8 copy-start.5
  6.5 2.9 copy-start.6
  6.5 2.9 copy-start.3
  6.5 3.0 copy-start.4
  6.5 52.0 %all-gather.8.cloned.1.call-start = ((), (), s32[]{:S(2)}) async-start(), calls=%async_computation | async-start | bytes 4718592 | tf_op jit(solution)/shard_map/all_gather | solution.py:28
  7.3 139.5 %all-gather.12.cloned.1.call-start = ((), (), s32[]{:S(2)}) async-start(), calls=%async_computation.2 | async-start | bytes 10485760 | tf_op jit(solution)/shard_map/all_gather | solution.py:23
  8.0 228.1 %all-gather.10.cloned.1.call-start = ((), (), s32[]{:S(2)}) async-start(), calls=%async_computation.1 | async-start | bytes 10485760 | tf_op jit(solution)/shard_map/all_gather | solution.py:22
  8.8 316.6 %all-gather.16.cloned.1.call-start = ((), (), s32[]{:S(2)}) async-start(), calls=%async_computation.4 | async-start | bytes 10485760 | tf_op jit(solution)/shard_map/all_gather | solution.py:24
  9.3 364.3 %all-gather.14.cloned.1.call-start = ((), (), s32[]{:S(2)}) async-start(), calls=%async_computation.3 | async-start | bytes 4718592 | tf_op jit(solution)/shard_map/all_gather | solution.py:55
  152.7 92.6 %copy-start.7 = (f32[2,512]{1,0:T(2,128)S(1)}, f32[2,512]{1,0:T(2,128)}, u32[]{:S(2)}) copy-start(f32[2,512]{1,0:T(2,128)} %param.16) | copy-start | bytes 12292
  242.0 5.0 collective-permute-start
  247.1 21.7 %copy-start.8 = (f32[2,512]{1,0:T(2,128)S(1)}, f32[2,512]{1,0:T(2,128)}, u32[]{:S(2)}) copy-start(f32[2,512]{1,0:T(2,128)} %param.19) | copy-start | bytes 12292
  268.7 171.8 %all-gather.18.cloned.1.call-start = ((), (), s32[]{:S(2)}) async-start(), calls=%async_computation.5 | async-start | bytes 4718592 | tf_op jit(solution)/shard_map/all_gather | solution.py:28
  268.8 125.7 %copy-start.2 = (bf16[512,512]{1,0:T(8,128)(2,1)S(1)}, bf16[512,512]{1,0:T(8,128)(2,1)}, u32[]{:S(2)}) copy-start(bf16[512,512]{1,0:T(8,128)(2,1)} %param.10) | copy-start | bytes 1572868
  395.5 127.0 %all-gather.20.cloned.1.call-start = ((), (), s32[]{:S(2)}) async-start(), calls=%async_computation.6 | async-start | bytes 4718592 | tf_op jit(solution)/shard_map/all_gather | solution.py:55
  440.5 3.4 copy-start.1
  440.5 8.5 %slice-start = ((s8[8388608]{0:T(1024)(128)(4,1)}), s8[4194304]{0:T(1024)(128)(4,1)S(1)}, s32[]{:S(2)}) async-start(s8[8388608]{0:T(1024)(128)(4,1)} %bitcast.194), calls=%async_computation.7 | async-start | bytes 8388608
  443.9 5.0 slice-start.1
  451.4 5.0 collective-permute-start.1
  476.6 66.7 %copy-start = (bf16[512,512]{1,0:T(8,128)(2,1)S(1)}, bf16[512,512]{1,0:T(8,128)(2,1)}, u32[]{:S(2)}) copy-start(bf16[512,512]{1,0:T(8,128)(2,1)} %fusion.33) | copy-start | bytes 1572868
Sparse Core Ops, SparseCore 0:
  9.0 49.5 all-gather.7
  60.4 86.2 all-gather.11
  148.6 87.4 all-gather.9
  237.8 87.4 all-gather.15
  326.8 46.8 all-gather.13
  395.7 44.7 all-gather.17
  476.7 45.7 all-gather.19
where the time goes:
time: 551 us
  waiting for transfers between devices  419 us (76%)
  blocking collectives  58.7 us (11%)
  matrix products  30.8 us (6%)
  other arithmetic  21.7 us (4%)
  between operations  13.8 us (3%)
  starting transfers between devices  7.2 us (1%)
    all_gather x2, waiting for transfers between devices, shards(): whole_mixed = lax.all_gather(mixed, 'tp', axis=1, tiled=True)  94.2 us
    all_gather x2, waiting for transfers between devices, shards(): gathered = lax.all_gather(stream, 'tp', axis=1, tiled=True)  93.7 us
    all_gather x1, waiting for transfers between devices, shards(): lax.all_gather(w_gate, 'sp', axis=1, tiled=True)  85.1 us
    all_gather x1, waiting for transfers between devices, shards(): lax.all_gather(w_value, 'sp', axis=1, tiled=True)  83.4 us
    all_gather x1, waiting for transfers between devices, shards(): lax.all_gather(w_out, 'sp', axis=1, tiled=True)  56.5 us
    psum x2, blocking collectives, shards(): total = lax.psum(jnp.sum(branch * branch, axis=-1), 'tp')  29.6 us
    psum x2, blocking collectives, shards(): lax.psum((jnp.sum(filtered, axis=-1), jnp.sum(filtered * filtered, axis=-...  29.1 us
    dot_general x2, matrix products, shards(): jnp.dot(whole_mixed, out_block, preferred_element_type=jnp.float32)  11.6 us
  transfers between devices with their start and end apart: 9, of which 9 were waited for; matrix products, arithmetic and copies ran while one was open for 4% of the time, Pallas kernels for 0%

commit v1 on v0

--- a/solution.py
+++ b/solution.py
@@ -25,7 +25,7 @@
     )
     stream = tokens
     for layer_index in range(layer_count):
-        gathered = lax.all_gather(stream, "tp", axis=1, tiled=True)
+        gathered = jnp.concatenate(lax.all_gather(stream, "tp"), axis=1)
         full_rows = gathered.astype(jnp.float32)
         scale_rows = lax.rsqrt(jnp.mean(full_rows * full_rows, axis=-1, keepdims=True) + 1e-06)
         normed = (full_rows * scale_rows * pre_gain[layer_index]).astype(jnp.bfloat16)

time: 551 us -> 569 us (1.033)
  local copies, waits for them, and re-layouts: 0.46 us -> 16.7 us
  other arithmetic: 21.7 us -> 33.5 us
  waiting for transfers between devices: 419 us -> 408 us
    convert_element_type x0 -> x2, local copies, waits for them, and re-layouts: none -> 16 us  [the longest x1 9.11 us: shards(): full_rows = gathered.astype(jnp.float32)]
    convert_element_type x0 -> x3, other arithmetic: none -> 11.7 us  [the longest x2 7.35 us: shards(): (full_rows * scale_rows * pre_gain[layer_index]).astype(jnp.bfloat16)]
    all_gather x1, waiting for transfers between devices: 85.1 us -> 74.6 us  [shards(): lax.all_gather(w_gate, 'sp', axis=1, tiled=True)]
  transfers between devices with their start and end apart: 9 -> 9, of which waited for: 9 -> 9; matrix products, arithmetic and copies ran while one was open for 4% -> 6% of each run, Pallas kernels for 0% -> 0%
where the time goes in v1:
time: 569 us; the launch traced here: 568 us
  waiting for transfers between devices  408 us (72%)
  blocking collectives  58.7 us (10%)
  other arithmetic  33.5 us (6%)
  matrix products  30.5 us (5%)
  local copies, waits for them, and re-layouts  16.7 us (3%)
  between operations  13.8 us (2%)
  starting transfers between devices  7.2 us (1%)
    all_gather x2, waiting for transfers between devices, shards(): whole_mixed = lax.all_gather(mixed, 'tp', axis=1, tiled=True)  94.2 us
    all_gather x2, waiting for transfers between devices, shards(): gathered = jnp.concatenate(lax.all_gather(stream, 'tp'), axis=1)  93.6 us
    all_gather x1, waiting for transfers between devices, shards(): lax.all_gather(w_value, 'sp', axis=1, tiled=True)  83.4 us
    all_gather x1, waiting for transfers between devices, shards(): lax.all_gather(w_gate, 'sp', axis=1, tiled=True)  74.6 us
    all_gather x1, waiting for transfers between devices, shards(): lax.all_gather(w_out, 'sp', axis=1, tiled=True)  56.6 us
    psum x2, blocking collectives, shards(): total = lax.psum(jnp.sum(branch * branch, axis=-1), 'tp')  29.6 us
    psum x2, blocking collectives, shards(): lax.psum((jnp.sum(filtered, axis=-1), jnp.sum(filtered * filtered, axis=-...  29.1 us
    dot_general x2, matrix products, shards(): jnp.dot(whole_mixed, out_block, preferred_element_type=jnp.float32)  11.6 us
  transfers between devices with their start and end apart: 9, of which 9 were waited for; matrix products, arithmetic and copies ran while one was open for 6% of the time, Pallas kernels for 0%

profile of v1, /device:TPU:0, one launch (start us, length us, event | category | flops | bytes accessed | tf_op | source)
XLA Modules:
  0.0 568.5 jit_solution(5599667281327966905)
XLA Ops:
  6.5 0.0 all-gather.20.cloned.1.call-start
  6.6 0.7 all-gather.20.cloned.1.call-update
  7.3 0.0 all-gather.12.cloned.1.call-start
  7.3 0.7 all-gather.12.cloned.1.call-update
  8.0 0.0 all-gather.10.cloned.1.call-start
  8.1 0.7 all-gather.10.cloned.1.call-update
  8.8 0.0 all-gather.16.cloned.1.call-start
  8.8 0.5 all-gather.16.cloned.1.call-update
  9.3 0.0 all-gather.14.cloned.1.call-start
  9.4 0.1 slice_reduce_fusion
  9.5 0.0 copy-done.6
  9.7 48.9 %all-gather.20.cloned.1.call-done = bf16[4096,512]{1,0:T(8,128)(2,1)} async-done(((bf16[512,512]{1,0:T(8,128)(2,1)}), bf16[4096,512]{1,0:T(8,128)(2,1)}) %all-gather.20.cloned.1.call-update) | async-done | bytes 4194320 | tf_op jit(solution)/shard_map/all_gather | solution.py:28
  58.6 3.2 fusion
  61.8 0.2 copy-done.1
  62.0 3.3 fusion.3
  65.3 6.8 %copy.12 = bf16[512,8,512]{0,2,1:T(8,128)(2,1)} copy(bf16[512,8,512]{2,0,1:T(8,128)(2,1)} %fusion.3) | data formatting | bytes 8388608 | tf_op jit(solution)/shard_map/convert_element_type | solution.py:31
  72.1 74.6 %all-gather.12.cloned.1.call-done = bf16[2,4096,512]{2,1,0:T(8,128)(2,1)} async-done(((bf16[2,1024,512]{2,1,0:T(8,128)(2,1)}), bf16[2,4096,512]{2,1,0:T(8,128)(2,1)}) %all-gather.12.cloned.1.call-update) | async-done | bytes 8388624 | tf_op jit(solution)/shard_map/all_gather | solution.py:23
  146.7 6.0 %fusion.19 = f32[512,512]{1,0:T(8,128)S(1)} fusion(bf16[512,4096]{0,1:T(8,128)(2,1)} %bitcast.136, bf16[2,4096,512]{2,1,0:T(8,128)(2,1)} %all-gather.12.cloned.1.call-done), kind=kOutput, calls=%fused_computation.33 | convolution fusion | flops 2148270080 | bytes 9437184 | tf_op jit(solution)/shard_map/dot_general | solution.py:36
  152.7 0.0 copy-start.8
  152.7 83.4 %all-gather.10.cloned.1.call-done = bf16[2,4096,512]{2,1,0:T(8,128)(2,1)} async-done(((bf16[2,1024,512]{2,1,0:T(8,128)(2,1)}), bf16[2,4096,512]{2,1,0:T(8,128)(2,1)}) %all-gather.10.cloned.1.call-update) | async-done | bytes 8388624 | tf_op jit(solution)/shard_map/all_gather | solution.py:22
  236.1 5.8 %fusion.21 = bf16[512,512]{1,0:T(8,128)(2,1)S(1)} fusion(f32[512,512]{1,0:T(8,128)S(1)} %fusion.19, bf16[512,4096]{0,1:T(8,128)(2,1)} %bitcast.137, bf16[2,4096,512]{2,1,0:T(8,128)(2,1)} %all-gather.10.cloned.1.call-done), kind=kOutput, calls=%fused_computation.35 | convolution fusion | flops 2148007936 | bytes 9961472 | tf_op jit(solution)/shard_map/dot_general | solution.py:35
  241.9 3.4 collective-permute-start
  245.3 1.6 collective-permute-done
  246.9 0.2 maximum_convert_fusion
  247.1 0.0 copy-start.9
  247.1 5.0 fusion.95
  252.1 15.3 %all-reduce.1 = (f32[512]{0:T(512)S(1)}, f32[512]{0:T(512)S(1)}) all-reduce(f32[512]{0:T(512)S(1)} %get-tuple-element.8, f32[512]{0:T(512)S(1)} %get-tuple-element.7), channel_id=1, replica_groups=mesh['sp'=4,'tp'=8] {'tp'}, use_global_device_ids=true, to_apply=%region_4.0 | all-reduce | flops 1024 | bytes 8192 | tf_op jit(solution)/shard_map/psum | solution.py:46
  267.4 1.2 multiply_convert_fusion.2
  268.6 0.0 all-gather.14.cloned.1.call-update
  268.7 0.0 all-gather.22.cloned.1.call-start
  268.7 0.0 copy-start.3
  268.7 56.6 %all-gather.16.cloned.1.call-done = bf16[2,4096,512]{2,1,0:T(8,128)(2,1)} async-done(((bf16[2,1024,512]{2,1,0:T(8,128)(2,1)}), bf16[2,4096,512]{2,1,0:T(8,128)(2,1)}) %all-gather.16.cloned.1.call-update) | async-done | bytes 8388624 | tf_op jit(solution)/shard_map/all_gather | solution.py:24
  325.3 48.4 %all-gather.14.cloned.1.call-done = bf16[512,4096]{1,0:T(8,128)(2,1)} async-done(((bf16[512,512]{1,0:T(8,128)(2,1)}), bf16[512,4096]{1,0:T(8,128)(2,1)}) %all-gather.14.cloned.1.call-update) | async-done | bytes 4194320 | tf_op jit(solution)/shard_map/all_gather | solution.py:55
  373.7 5.8 %fusion.22 = bf16[512,512]{1,0:T(8,128)(2,1)S(1)} fusion(bf16[512,4096]{1,0:T(8,128)(2,1)} %all-gather.14.cloned.1.call-done, bf16[2,4096,512]{2,1,0:T(8,128)(2,1)} %all-gather.16.cloned.1.call-done), kind=kOutput, calls=%fused_computation.36 | convolution fusion | flops 2147745792 | bytes 8912896 | tf_op jit(solution)/shard_map/dot_general | solution.py:56
  379.4 0.2 fusion.24
  379.6 14.8 %psum.44 = f32[512]{0:T(512)S(1)} all-reduce(f32[512]{0:T(512)S(1)} %fusion.24), channel_id=1, replica_groups=mesh['sp'=4,'tp'=8] {'tp'}, use_global_device_ids=true, to_apply=%region_6.7 | all-reduce | flops 512 | bytes 4096 | tf_op jit(solution)/shard_map/psum | solution.py:60
  394.4 1.1 fusion.27
  395.5 0.0 all-gather.22.cloned.1.call-update
  395.5 0.2 all-gather.18.cloned.1.call-start
  395.8 44.7 %all-gather.22.cloned.1.call-done = bf16[4096,512]{1,0:T(8,128)(2,1)} async-done(((bf16[512,512]{1,0:T(8,128)(2,1)}), bf16[4096,512]{1,0:T(8,128)(2,1)}) %all-gather.22.cloned.1.call-update) | async-done | bytes 4194320 | tf_op jit(solution)/shard_map/all_gather | solution.py:28
  440.5 3.2 multiply_reduce_fusion
  443.7 0.2 copy-done
  443.9 4.4 bitcast_convert_fusion
  448.3 9.1 %copy.13 = f32[8,512,512]{1,2,0:T(8,128)} copy(f32[8,512,512]{2,1,0:T(8,128)} %bitcast_convert_fusion) | data formatting | bytes 16777216 | tf_op jit(solution)/shard_map/convert_element_type | solution.py:29
  457.4 4.1 multiply_convert_fusion
  461.5 0.0 slice-start.1
  461.5 4.8 fusion.17
  466.3 0.0 slice-done
  466.4 0.0 slice-done.1
  466.4 2.3 fusion.20
  468.7 3.4 collective-permute-start.1
  472.2 1.5 collective-permute-done.1
  473.7 0.2 maximum_convert_fusion.1
  473.9 5.0 fusion.94
  478.9 13.7 %all-reduce = (f32[512]{0:T(512)S(1)}, f32[512]{0:T(512)S(1)}) all-reduce(f32[512]{0:T(512)S(1)} %get-tuple-element.6, f32[512]{0:T(512)S(1)} %get-tuple-element.5), channel_id=1, replica_groups=mesh['sp'=4,'tp'=8] {'tp'}, use_global_device_ids=true, to_apply=%region_11.12 | all-reduce | flops 1024 | bytes 8192 | tf_op jit(solution)/shard_map/psum | solution.py:46
  492.6 1.2 multiply_convert_fusion.1
  493.9 0.0 all-gather.18.cloned.1.call-update
  493.9 0.0 copy-start.2
  493.9 45.9 %all-gather.18.cloned.1.call-done = bf16[512,4096]{1,0:T(8,128)(2,1)} async-done(((bf16[512,512]{1,0:T(8,128)(2,1)}), bf16[512,4096]{1,0:T(8,128)(2,1)}) %all-gather.18.cloned.1.call-update) | async-done | bytes 4194320 | tf_op jit(solution)/shard_map/all_gather | solution.py:55
  539.8 5.8 %fusion.23 = bf16[512,512]{1,0:T(8,128)(2,1)S(1)} fusion(bf16[512,4096]{1,0:T(8,128)(2,1)} %all-gather.18.cloned.1.call-done, bf16[2,4096,512]{2,1,0:T(8,128)(2,1)} %all-gather.16.cloned.1.call-done), kind=kOutput, calls=%fused_computation.37 | convolution fusion | flops 2147745792 | bytes 8912896 | tf_op jit(solution)/shard_map/dot_general | solution.py:56
  545.6 0.2 fusion.28
  545.7 14.8 %psum.47 = f32[512]{0:T(512)S(1)} all-reduce(f32[512]{0:T(512)S(1)} %fusion.28), channel_id=1, replica_groups=mesh['sp'=4,'tp'=8] {'tp'}, use_global_device_ids=true, to_apply=%region_13.14 | all-reduce | flops 512 | bytes 4096 | tf_op jit(solution)/shard_map/psum | solution.py:60
  560.6 0.0 copy-done.2
  560.6 1.1 fusion.31
  (32 shorter events, 0.3 us)
Async XLA Ops:
  6.5 2.8 copy-start.5
  6.5 3.0 copy-start.6
  6.5 3.0 copy-start.7
  6.5 3.0 copy-start.4
  6.5 52.0 %all-gather.20.cloned.1.call-start = ((), (), s32[]{:S(2)}) async-start(), calls=%async_computation.5 | async-start | bytes 4718592 | tf_op jit(solution)/shard_map/all_gather | solution.py:28
  7.3 139.5 %all-gather.12.cloned.1.call-start = ((), (), s32[]{:S(2)}) async-start(), calls=%async_computation.1 | async-start | bytes 10485760 | tf_op jit(solution)/shard_map/all_gather | solution.py:23
  8.0 228.1 %all-gather.10.cloned.1.call-start = ((), (), s32[]{:S(2)}) async-start(), calls=%async_computation | async-start | bytes 10485760 | tf_op jit(solution)/shard_map/all_gather | solution.py:22
  8.8 316.5 %all-gather.16.cloned.1.call-start = ((), (), s32[]{:S(2)}) async-start(), calls=%async_computation.3 | async-start | bytes 10485760 | tf_op jit(solution)/shard_map/all_gather | solution.py:24
  9.3 364.3 %all-gather.14.cloned.1.call-start = ((), (), s32[]{:S(2)}) async-start(), calls=%async_computation.2 | async-start | bytes 4718592 | tf_op jit(solution)/shard_map/all_gather | solution.py:55
  58.6 3.4 copy-start.1
  152.7 92.6 %copy-start.8 = (f32[2,512]{1,0:T(2,128)S(1)}, f32[2,512]{1,0:T(2,128)}, u32[]{:S(2)}) copy-start(f32[2,512]{1,0:T(2,128)} %param.17) | copy-start | bytes 12292
  241.9 5.0 collective-permute-start
  247.1 21.7 %copy-start.9 = (f32[2,512]{1,0:T(2,128)S(1)}, f32[2,512]{1,0:T(2,128)}, u32[]{:S(2)}) copy-start(f32[2,512]{1,0:T(2,128)} %param.19) | copy-start | bytes 12292
  268.7 171.8 %all-gather.22.cloned.1.call-start = ((), (), s32[]{:S(2)}) async-start(), calls=%async_computation.6 | async-start | bytes 4718592 | tf_op jit(solution)/shard_map/all_gather | solution.py:28
  268.7 125.7 %copy-start.3 = (bf16[512,512]{1,0:T(8,128)(2,1)S(1)}, bf16[512,512]{1,0:T(8,128)(2,1)}, u32[]{:S(2)}) copy-start(bf16[512,512]{1,0:T(8,128)(2,1)} %param.10) | copy-start | bytes 1572868
  395.5 144.2 %all-gather.18.cloned.1.call-start = ((), (), s32[]{:S(2)}) async-start(), calls=%async_computation.4 | async-start | bytes 4718592 | tf_op jit(solution)/shard_map/all_gather | solution.py:55
  440.5 3.4 copy-start
  457.4 8.9 %slice-start = ((s8[8388608]{0:T(1024)(128)(4,1)}), s8[4194304]{0:T(1024)(128)(4,1)S(1)}, s32[]{:S(2)}) async-start(s8[8388608]{0:T(1024)(128)(4,1)} %bitcast.210), calls=%async_computation.7 | async-start | bytes 8388608
  461.5 4.9 slice-start.1
  468.7 5.0 collective-permute-start.1
  493.9 66.7 %copy-start.2 = (bf16[512,512]{1,0:T(8,128)(2,1)S(1)}, bf16[512,512]{1,0:T(8,128)(2,1)}, u32[]{:S(2)}) copy-start(bf16[512,512]{1,0:T(8,128)(2,1)} %fusion.27) | copy-start | bytes 1572868
Sparse Core Ops, SparseCore 0:
  8.9 49.5 all-gather.19
  60.4 86.2 all-gather.11
  148.6 87.4 all-gather.9
  237.8 87.4 all-gather.15
  326.8 46.8 all-gather.13
  395.6 44.7 all-gather.21
  494.0 45.7 all-gather.17
